TPU v7x, 32 devices: a whole 2x2x4 slice. The times are simulated.
32 devices in a mesh: ep: 4 (over y, x), tp: 8 (over z, core).
Axes of the slice: x: 2, y: 2, z: 4, core: 2. Of those that a mesh axis runs over, the one named last changes fastest.
Arguments:
- tokens: bfloat16 [128, 4096], P('ep'), may hold values from -6 to 6
- state_matrix: float32 [128, 16, 128, 128], P('ep', 'tp'), may hold values from -1.5 to 1.5
- state_norm: float32 [128, 16, 128], P('ep', 'tp'), may hold values from -4 to 4
- state_max: float32 [128, 16], P('ep', 'tp'), may hold values from -5 to 5
- mixer_gain: float32 [4096], replicated, may hold values from 0.1 to 1.9
- w_query: bfloat16 [4096, 2048], P('ep', 'tp'), may hold values from -0.09375 to 0.09375
- w_key: bfloat16 [4096, 2048], P('ep', 'tp'), may hold values from -0.09375 to 0.09375
- w_value: bfloat16 [4096, 2048], P('ep', 'tp'), may hold values from -0.09375 to 0.09375
- w_outgate: bfloat16 [4096, 2048], P('ep', 'tp'), may hold values from -0.09375 to 0.09375
- w_ingate: bfloat16 [4096, 16], replicated, may hold values from -0.09375 to 0.09375
- w_forget: bfloat16 [4096, 16], replicated, may hold values from -0.09375 to 0.09375
- forget_bias: float32 [16], replicated, may hold values from -2 to 4
- w_proj: bfloat16 [2048, 4096], P('tp', 'ep'), may hold values from -0.125 to 0.125
- ffn_gain: float32 [4096], replicated, may hold values from 0.1 to 1.9
- w_branch: bfloat16 [4096], replicated, may hold values from -0.09375 to 0.09375
- routes: int32 [128, 2], P('ep'), may hold values from 0 to 3, all different within a row; in each aligned block of 32 rows (0 to 31, 32 to 63, ...) at most 22 rows name the same one
- route_weight: float32 [128, 2], P('ep'), may hold values from 0.2 to 1
- expert_gate: bfloat16 [4, 4096, 4096], P('ep', None, 'tp'), may hold values from -0.09375 to 0.09375
- expert_up: bfloat16 [4, 4096, 4096], P('ep', None, 'tp'), may hold values from -0.09375 to 0.09375
- expert_down: bfloat16 [4, 4096, 4096], P('ep', 'tp'), may hold values from -0.09375 to 0.09375
- dense_gate: bfloat16 [4096, 8192], P('ep', 'tp'), may hold values from -0.09375 to 0.09375
- dense_up: bfloat16 [4096, 8192], P('ep', 'tp'), may hold values from -0.09375 to 0.09375
- dense_down: bfloat16 [8192, 4096], P('tp', 'ep'), may hold values from -0.0625 to 0.0625
Outputs:
- layer_out: bfloat16 [128, 4096], P('ep')
- new_matrix: float32 [128, 16, 128, 128], P('ep', 'tp')
- new_norm: float32 [128, 16, 128], P('ep', 'tp')
- new_max: float32 [128, 16], P('ep', 'tp')
Inputs may be any that keep to these rules, and one draw needn't show every extreme that they name: `routes`: each row names 2 different experts. Among the rows of one index of ep (32 sequences) no expert is named more than 22 times, and in some such group one expert is named exactly 22 times.
All inputs are finite; a program needn't handle non-finite values.
Results may differ from a plain program's by a relative error of at most 0.012.
Values may be sent and summed in bfloat16 or wider, within the bound.
A program may use at most 64 MiB of HBM per device.

v0:
```python
import jax
import jax.numpy as jnp
from jax import lax
from jax.sharding import PartitionSpec as P

EPS = 1e-06


def rms_scale(values, gain):
    wide = values.astype(jnp.float32)
    return wide * lax.rsqrt(jnp.mean(wide * wide, axis=-1, keepdims=True) + EPS) * gain


def slot_numbers(flat_routes, experts_all):
    onehot = (flat_routes[:, None] == jnp.arange(experts_all, dtype=jnp.int32)[None, :]).astype(
        jnp.int32
    )
    before = jnp.cumsum(onehot, axis=0) - onehot
    return jnp.sum(before * onehot, axis=1)


def memory_step(
    query_all,
    key_all,
    value_all,
    outgate,
    gate_in,
    gate_forget,
    state_matrix,
    state_norm,
    state_max,
):
    row_count, head_count = gate_in.shape
    head_size = state_matrix.shape[-1]
    heads_q = query_all.reshape(row_count, head_count, head_size)
    heads_k = key_all.reshape(row_count, head_count, head_size) * head_size ** (-0.5)
    heads_v = value_all.reshape(row_count, head_count, head_size)
    log_keep = jax.nn.log_sigmoid(gate_forget)
    new_max = jnp.maximum(log_keep + state_max, gate_in)
    keep_factor = jnp.exp(log_keep + state_max - new_max)
    write_factor = jnp.exp(gate_in - new_max)
    new_matrix = (
        keep_factor[:, :, None, None] * state_matrix
        + write_factor[:, :, None, None] * heads_k[:, :, :, None] * heads_v[:, :, None, :]
    )
    new_norm = keep_factor[:, :, None] * state_norm + write_factor[:, :, None] * heads_k
    numer = jnp.einsum("bhk,bhkv->bhv", heads_q, new_matrix, precision=lax.Precision.HIGHEST)
    denom = jnp.sum(heads_q * new_norm, axis=-1)
    cell = numer / jnp.maximum(jnp.abs(denom), 1.0)[:, :, None]
    gated = jax.nn.sigmoid(outgate.reshape(row_count, head_count, head_size)) * cell
    mixed_heads = gated.reshape(row_count, head_count * head_size).astype(jnp.bfloat16)
    return (mixed_heads, new_matrix, new_norm, new_max)


def on_device(
    tokens,
    state_matrix,
    state_norm,
    state_max,
    mixer_gain,
    w_query,
    w_key,
    w_value,
    w_outgate,
    w_ingate,
    w_forget,
    forget_bias,
    w_proj,
    ffn_gain,
    w_branch,
    routes,
    route_weight,
    expert_gate,
    expert_up,
    expert_down,
    dense_gate,
    dense_up,
    dense_down,
):
    row_count = tokens.shape[0]
    head_count = state_matrix.shape[1]
    model_width = tokens.shape[1]
    normed = rms_scale(tokens, mixer_gain).astype(jnp.bfloat16)
    head_start = lax.axis_index("tp") * head_count
    gate_in = lax.dynamic_slice_in_dim(
        jnp.dot(normed, w_ingate, preferred_element_type=jnp.float32), head_start, head_count, 1
    )
    forget_all = jnp.dot(normed, w_forget, preferred_element_type=jnp.float32) + forget_bias
    gate_forget = lax.dynamic_slice_in_dim(forget_all, head_start, head_count, 1)
    spread = lax.all_to_all(normed, "ep", split_axis=1, concat_axis=0, tiled=True)
    part_q = jnp.dot(spread, w_query, preferred_element_type=jnp.float32)
    part_k = jnp.dot(spread, w_key, preferred_element_type=jnp.float32)
    part_v = jnp.dot(spread, w_value, preferred_element_type=jnp.float32)
    part_o = jnp.dot(spread, w_outgate, preferred_element_type=jnp.float32)
    projected = (
        lax.psum_scatter(part_q, "ep", scatter_dimension=0, tiled=True),
        lax.psum_scatter(part_k, "ep", scatter_dimension=0, tiled=True),
        lax.psum_scatter(part_v, "ep", scatter_dimension=0, tiled=True),
        lax.psum_scatter(part_o, "ep", scatter_dimension=0, tiled=True),
    )
    mixed_heads, new_matrix, new_norm, new_max = memory_step(
        projected[0],
        projected[1],
        projected[2],
        projected[3],
        gate_in,
        gate_forget,
        state_matrix,
        state_norm,
        state_max,
    )
    spread_out = jnp.dot(
        lax.all_gather(mixed_heads, "ep", axis=0, tiled=True),
        w_proj,
        preferred_element_type=jnp.float32,
    )
    mix_back = lax.all_to_all(spread_out, "ep", split_axis=0, concat_axis=1, tiled=True)
    mixer_out = lax.psum(mix_back, "tp")
    residual = (tokens.astype(jnp.float32) + mixer_out).astype(jnp.bfloat16)
    ffn_in = rms_scale(residual, ffn_gain).astype(jnp.bfloat16)
    branch_share = jax.nn.sigmoid(jnp.dot(ffn_in, w_branch, preferred_element_type=jnp.float32))
    dense_spread = lax.all_to_all(ffn_in, "ep", split_axis=1, concat_axis=0, tiled=True)
    dense_g, dense_u = (
        lax.psum_scatter(
            jnp.dot(dense_spread, dense_gate, preferred_element_type=jnp.float32),
            "ep",
            scatter_dimension=0,
            tiled=True,
        ),
        lax.psum_scatter(
            jnp.dot(dense_spread, dense_up, preferred_element_type=jnp.float32),
            "ep",
            scatter_dimension=0,
            tiled=True,
        ),
    )
    dense_hidden = (jax.nn.silu(dense_g) * dense_u).astype(jnp.bfloat16)
    dense_spread_out = jnp.dot(
        lax.all_gather(dense_hidden, "ep", axis=0, tiled=True),
        dense_down,
        preferred_element_type=jnp.float32,
    )
    dense_back = lax.all_to_all(dense_spread_out, "ep", split_axis=0, concat_axis=1, tiled=True)
    ep_count = lax.axis_size("ep")
    local_experts = expert_gate.shape[0]
    experts_all = local_experts * ep_count
    top_count = routes.shape[1]
    capacity = max(2, (row_count * top_count * 4 + 3 * experts_all - 1) // (3 * experts_all))
    flat_routes = routes.reshape(-1)
    slots = slot_numbers(flat_routes, experts_all)
    outbound = (
        jnp.zeros((experts_all, capacity, model_width), jnp.bfloat16)
        .at[flat_routes, slots]
        .set(jnp.repeat(ffn_in, top_count, axis=0))
    )
    arrived = lax.all_to_all(outbound, "ep", split_axis=0, concat_axis=0, tiled=True)
    slot_count = arrived.shape[1]
    grid = arrived.reshape(ep_count, local_experts, slot_count, model_width)
    gate_part = jnp.einsum("secd,edf->secf", grid, expert_gate, preferred_element_type=jnp.float32)
    up_part = jnp.einsum("secd,edf->secf", grid, expert_up, preferred_element_type=jnp.float32)
    hidden = (jax.nn.silu(gate_part) * up_part).astype(jnp.bfloat16)
    partial_out = jnp.einsum(
        "secf,efd->secd", hidden, expert_down, preferred_element_type=jnp.float32
    )
    partial_out = partial_out.reshape(ep_count * local_experts, slot_count, partial_out.shape[3])
    returned = lax.all_to_all(partial_out, "ep", split_axis=0, concat_axis=0, tiled=True)
    picked = returned[flat_routes, slots].reshape(row_count, top_count, returned.shape[2])
    shares = route_weight / jnp.sum(route_weight, axis=1, keepdims=True)
    expert_rows = jnp.sum(shares[:, :, None] * picked, axis=1)
    total_ffn = lax.psum(expert_rows + branch_share[:, None] * dense_back, "tp")
    layer_out = (residual.astype(jnp.float32) + total_ffn).astype(jnp.bfloat16)
    return (layer_out, new_matrix, new_norm, new_max)


def solution(mesh):
    in_specs = (
        P("ep", None),
        P("ep", "tp", None, None),
        P("ep", "tp", None),
        P("ep", "tp"),
        P(),
        P("ep", "tp"),
        P("ep", "tp"),
        P("ep", "tp"),
        P("ep", "tp"),
        P(),
        P(),
        P(),
        P("tp", "ep"),
        P(),
        P(),
        P("ep", None),
        P("ep", None),
        P("ep", None, "tp"),
        P("ep", None, "tp"),
        P("ep", "tp", None),
        P("ep", "tp"),
        P("ep", "tp"),
        P("tp", "ep"),
    )
    out_specs = (P("ep", None), P("ep", "tp", None, None), P("ep", "tp", None), P("ep", "tp"))
    return jax.shard_map(
        on_device, mesh=mesh, in_specs=in_specs, out_specs=out_specs, check_vma=False
    )
```

profile of v0, /device:TPU:0, one launch (start us, length us, event | category | flops | bytes accessed | tf_op | source)
XLA Modules:
  0.0 382.4 jit_solution(11826097825616217500)
XLA Ops:
  7.2 1.3 fusion.27
  8.5 1.1 fusion.29
  10.3 5.2 %all-to-all-start = ((bf16[32,4,1024]{2,0,1:T(8,128)(2,1)}), bf16[32,4,1024]{2,0,1:T(8,128)(2,1)S(1)}, u32[]{:S(2)}, u32[]{:S(2)}) async-start(bf16[32,4,1024]{2,0,1:T(8,128)(2,1)} %bitcast.121), calls=%async_computation | async-start | bytes 524288 | tf_op jit(solution)/shard_map/all_to_all | solution.py:90
  15.5 1.1 fusion.54
  16.6 4.3 %all-to-all-done = bf16[32,4,1024]{2,0,1:T(8,128)(2,1)S(1)} async-done(((bf16[32,4,1024]{2,0,1:T(8,128)(2,1)}), bf16[32,4,1024]{2,0,1:T(8,128)(2,1)S(1)}, u32[]{:S(2)}, u32[]{:S(2)}) %all-to-all-start) | async-done | bytes 262176 | tf_op jit(solution)/shard_map/all_to_all | solution.py:90
  20.9 1.9 fusion.52
  22.9 1.1 fusion.53
  24.7 1.9 fusion.55
  26.8 0.9 fusion.51
  28.0 1.9 fusion.56
  30.0 17.2 %reduce-scatter.9.cloned.1.call-done = f32[32,256]{1,0:T(8,128)} async-done(((f32[128,256]{1,0:T(8,128)}), f32[32,256]{1,0:T(8,128)}) %reduce-scatter.9.cloned.1.call-update) | async-done | bytes 32784 | tf_op jit(solution)/shard_map/reduce_scatter | solution.py:96
  47.2 0.8 reshape.146
  48.0 26.1 %reduce-scatter.11.cloned.1.call-done = f32[32,256]{1,0:T(8,128)} async-done(((f32[128,256]{1,0:T(8,128)}), f32[32,256]{1,0:T(8,128)}) %reduce-scatter.11.cloned.1.call-update) | async-done | bytes 32784 | tf_op jit(solution)/shard_map/reduce_scatter | solution.py:97
  75.6 25.9 %reduce-scatter.7.cloned.1.call-done = f32[32,256]{1,0:T(8,128)} async-done(((f32[128,256]{1,0:T(8,128)}), f32[32,256]{1,0:T(8,128)}) %reduce-scatter.7.cloned.1.call-update) | async-done | bytes 32784 | tf_op jit(solution)/shard_map/reduce_scatter | solution.py:99
  102.4 25.9 %reduce-scatter.13.cloned.1.call-done = f32[32,256]{1,0:T(8,128)} async-done(((f32[128,256]{1,0:T(8,128)}), f32[32,256]{1,0:T(8,128)}) %reduce-scatter.13.cloned.1.call-update) | async-done | bytes 32784 | tf_op jit(solution)/shard_map/reduce_scatter | solution.py:98
  129.1 4.3 %multiply_add_fusion = f32[32,2,128,128]{3,2,1,0:T(8,128)} fusion(f32[32,2,128,128]{3,2,1,0:T(8,128)} %param.24, f32[32,2,128]{2,1,0:T(2,128)S(1)} %mul.148, f32[32,2,128]{2,1,0:T(2,128)S(1)} %get-tuple-element.8, f32[32,2]{1,0:T(8,128)S(1)} %copy.60), kind=kLoop, calls=%fused_computation.8 | loop fusion | flops 3145728 | bytes 8454400 | tf_op jit(solution)/shard_map/add | solution.py:43
  133.5 5.3 %fusion.57 = f32[32,2,1,128]{3,2,1,0:T(1,128)S(1)} fusion(f32[32,2,128,1]{2,3,1,0:T(1,128)S(1)} %bitcast.137, f32[32,2,128,128]{3,2,1,0:T(8,128)} %multiply_add_fusion), kind=kOutput, calls=%fused_computation.80 | convolution fusion | flops 12582912 | bytes 4259840 | tf_op jit(solution)/shard_map/bhk,bhkv->bhv/dot_general | solution.py:47
  139.0 8.2 %all_gather.6 = bf16[128,256]{1,0:T(8,128)(2,1)S(1)} all-gather(bf16[32,256]{1,0:T(8,128)(2,1)S(1)} %bitcast.138), channel_id=1, replica_groups=mesh['ep'=4,'tp'=8] {'ep'}, dimensions={0}, use_global_device_ids=true | all-gather | bytes 81920 | tf_op jit(solution)/shard_map/all_gather | solution.py:113
  147.4 9.7 %all_to_all.86 = f32[4,32,1024]{2,1,0:T(8,128)S(1)} all-to-all(f32[4,32,1024]{2,1,0:T(8,128)S(1)} %bitcast.134), channel_id=1, replica_groups=mesh['ep'=4,'tp'=8] {'ep'}, dimensions={0} | all-to-all | bytes 1048576 | tf_op jit(solution)/shard_map/all_to_all | solution.py:117
  157.1 0.8 copy.75
  157.9 56.1 %all-reduce.3.cloned.1.call-done = f32[32,4096]{1,0:T(8,128)} async-done(((f32[32,4096]{1,0:T(8,128)}), f32[32,4096]{1,0:T(8,128)}) %all-reduce.3.cloned.1.call-update) | async-done | bytes 524304 | tf_op jit(solution)/shard_map/psum | solution.py:118
  214.1 1.2 fusion.31
  216.2 3.6 all-to-all-start.4
  220.1 5.1 %all-to-all-done.4 = bf16[32,4,1024]{2,0,1:T(8,128)(2,1)S(1)} async-done(((bf16[32,4,1024]{2,0,1:T(8,128)(2,1)}), bf16[32,4,1024]{2,0,1:T(8,128)(2,1)S(1)}, u32[]{:S(2)}, u32[]{:S(2)}) %all-to-all-start.4) | async-done | bytes 262176 | tf_op jit(solution)/shard_map/all_to_all | solution.py:122
  225.2 1.2 fusion.60
  226.8 1.3 broadcast_in_dim.5
  228.1 2.0 reshape.163
  230.4 13.2 %scatter_fusion = bf16[4,22,4096]{2,0,1:T(4,128)(2,1)S(1)} fusion(bf16[4,22,4096]{2,0,1:T(4,128)(2,1)S(1)} %broadcast_in_dim.4, s32[64]{0:T(128)S(1)} %get-tuple-element.11, bf16[64,4096]{1,0:T(8,128)(2,1)} %reshape.163), kind=kCustom, calls=%fused_computation.1 | custom fusion | bytes 1573376 | tf_op jit(solution)/shard_map/scatter | solution.py:154
  243.7 1.3 copy.67
  245.0 3.5 all-to-all-start.2
  248.5 2.9 fusion.59
  251.4 5.5 %all-to-all-done.2 = bf16[4,22,4096]{2,1,0:T(8,128)(2,1)S(1)} async-done(((bf16[4,22,4096]{2,1,0:T(8,128)(2,1)}), bf16[4,22,4096]{2,1,0:T(8,128)(2,1)S(1)}, u32[]{:S(2)}, u32[]{:S(2)}) %all-to-all-start.2) | async-done | bytes 720928 | tf_op jit(solution)/shard_map/all_to_all | solution.py:156
  256.9 3.0 fusion.6
  259.9 6.3 %fusion = f32[4,22,4096]{2,1,0:T(8,128)} fusion(bf16[1,512,4096]{2,1,0:T(8,128)(2,1)} %param.42, bf16[4,22,4096]{2,1,0:T(8,128)(2,1)S(1)} %all-to-all-done.2, bf16[1,4096,512]{2,1,0:T(8,128)(2,1)} %param.41, f32[4,1,22,512]{3,2,0,1:T(8,128)S(1)} %fusion.6), kind=kOutput, calls=%fused_computation.2 | convolution fusion | flops 738467840 | bytes 10731520 | tf_op jit(solution)/shard_map/secf,efd->secd/dot_general | solution.py:162
  266.3 4.3 %all-to-all-start.3 = ((f32[4,22,4096]{2,1,0:T(8,128)}), f32[4,22,4096]{2,1,0:T(8,128)}, u32[]{:S(2)}, u32[]{:S(2)}) async-start(f32[4,22,4096]{2,1,0:T(8,128)} %fusion), calls=%async_computation.7 | async-start | bytes 3145728 | tf_op jit(solution)/shard_map/all_to_all | solution.py:166
  271.4 11.0 %reduce-scatter.15.cloned.1.call-done = f32[32,1024]{1,0:T(8,128)} async-done(((f32[128,1024]{1,0:T(8,128)}), f32[32,1024]{1,0:T(8,128)}) %reduce-scatter.15.cloned.1.call-update) | async-done | bytes 131088 | tf_op jit(solution)/shard_map/reduce_scatter | solution.py:124
  282.3 1.0 multiply_convert_fusion
  283.4 8.9 %all_gather.7 = bf16[128,1024]{1,0:T(8,128)(2,1)S(1)} all-gather(bf16[32,1024]{1,0:T(8,128)(2,1)S(1)} %multiply_convert_fusion), channel_id=1, replica_groups=mesh['ep'=4,'tp'=8] {'ep'}, dimensions={0}, use_global_device_ids=true | all-gather | bytes 327680 | tf_op jit(solution)/shard_map/all_gather | solution.py:139
  292.2 2.8 fusion.61
  295.1 4.1 %all-to-all-start.5 = ((f32[4,32,1024]{2,1,0:T(8,128)}), f32[4,32,1024]{2,1,0:T(8,128)}, u32[]{:S(2)}, u32[]{:S(2)}) async-start(f32[4,32,1024]{2,1,0:T(8,128)} %bitcast.30), calls=%async_computation.11 | async-start | bytes 1048576 | tf_op jit(solution)/shard_map/all_to_all | solution.py:143
  299.5 2.4 copy.68
  301.8 3.1 gather_fusion
  304.9 1.9 reshape.154
  306.8 3.0 multiply_reduce_fusion
  309.8 1.1 copy.76
  310.8 2.0 multiply_add_fusion.1
  312.8 60.9 %all-reduce.5.cloned.1.call-done = f32[32,4096]{1,0:T(8,128)} async-done(((f32[32,4096]{1,0:T(8,128)}), f32[32,4096]{1,0:T(8,128)}) %all-reduce.5.cloned.1.call-update) | async-done | bytes 524304 | tf_op jit(solution)/shard_map/psum | solution.py:170
  373.7 1.8 fusion.34
  (80 shorter events, 8.4 us)
Async XLA Ops:
  7.2 218.0 %copy-start = (bf16[1024,1024]{1,0:T(8,128)(2,1)S(1)}, bf16[1024,1024]{1,0:T(8,128)(2,1)}, u32[]{:S(2)}) copy-start(bf16[1024,1024]{1,0:T(8,128)(2,1)} %param.44) | copy-start | bytes 6291460
  7.2 19.5 %copy-start.13 = (f32[32,2]{0,1:T(2,128)S(1)}, f32[32,2]{0,1:T(2,128)}, u32[]{:S(2)}) copy-start(f32[32,2]{0,1:T(2,128)} %param.26) | copy-start | bytes 772
  7.2 19.6 %copy-start.4 = (bf16[1024,256]{1,0:T(8,128)(2,1)S(1)}, bf16[1024,256]{1,0:T(8,128)(2,1)}, u32[]{:S(2)}) copy-start(bf16[1024,256]{1,0:T(8,128)(2,1)} %param.31) | copy-start | bytes 1572868
  7.2 67.7 %copy-start.7 = (f32[32,2,128]{2,1,0:T(2,128)S(1)}, f32[32,2,128]{2,1,0:T(2,128)}, u32[]{:S(2)}) copy-start(f32[32,2,128]{2,1,0:T(2,128)} %param.25) | copy-start | bytes 98308
  10.3 10.6 %all-to-all-start = ((bf16[32,4,1024]{2,0,1:T(8,128)(2,1)}), bf16[32,4,1024]{2,0,1:T(8,128)(2,1)S(1)}, u32[]{:S(2)}, u32[]{:S(2)}) async-start(bf16[32,4,1024]{2,0,1:T(8,128)(2,1)} %bitcast.121), calls=%async_computation | async-start | bytes 524288 | tf_op jit(solution)/shard_map/all_to_all | solution.py:90
  15.5 31.7 %reduce-scatter.9.cloned.1.call-start = ((), (), s32[]{:S(2)}) async-start(), calls=%async_computation.13 | async-start | bytes 163840 | tf_op jit(solution)/shard_map/reduce_scatter | solution.py:96
  22.8 51.3 %reduce-scatter.11.cloned.1.call-start = ((), (), s32[]{:S(2)}) async-start(), calls=%async_computation.14 | async-start | bytes 163840 | tf_op jit(solution)/shard_map/reduce_scatter | solution.py:97
  26.6 74.9 %reduce-scatter.7.cloned.1.call-start = ((), (), s32[]{:S(2)}) async-start(), calls=%async_computation.12 | async-start | bytes 163840 | tf_op jit(solution)/shard_map/reduce_scatter | solution.py:99
  26.8 106.7 %copy-start.11 = (f32[32,2]{0,1:T(2,128)}, f32[32,2]{0,1:T(2,128)S(1)}, u32[]{:S(2)}) copy-start(f32[32,2]{0,1:T(2,128)S(1)} %get-tuple-element.10) | copy-start | bytes 772
  27.7 100.6 %reduce-scatter.13.cloned.1.call-start = ((), (), s32[]{:S(2)}) async-start(), calls=%async_computation.15 | async-start | bytes 163840 | tf_op jit(solution)/shard_map/reduce_scatter | solution.py:98
  29.9 184.1 %all-reduce.3.cloned.1.call-start = ((), (), s32[]{:S(2)}) async-start(), calls=%async_computation.16 | async-start | bytes 1048576 | tf_op jit(solution)/shard_map/psum | solution.py:118
  129.1 4.3 %copy-start.6 = (f32[32,256]{1,0:T(8,128)S(1)}, f32[32,256]{1,0:T(8,128)}, u32[]{:S(2)}) copy-start(f32[32,256]{1,0:T(8,128)} %reduce-scatter.9.cloned.1.call-done) | copy-start | bytes 98308
  133.5 13.7 %copy-start.5 = (bf16[256,1024]{1,0:T(8,128)(2,1)S(1)}, bf16[256,1024]{1,0:T(8,128)(2,1)}, u32[]{:S(2)}) copy-start(bf16[256,1024]{1,0:T(8,128)(2,1)} %param.35) | copy-start | bytes 1572868
  133.5 80.6 %copy-start.1 = (bf16[32,4096]{1,0:T(8,128)(2,1)S(1)}, bf16[32,4096]{1,0:T(8,128)(2,1)}, u32[]{:S(2)}) copy-start(bf16[32,4096]{1,0:T(8,128)(2,1)} %param.23) | copy-start | bytes 786436
  133.5 81.8 %copy-start.8 = (f32[4096]{0:T(1024)S(1)}, f32[4096]{0:T(1024)}, u32[]{:S(2)}) copy-start(f32[4096]{0:T(1024)} %param.36) | copy-start | bytes 49156
  138.9 81.0 %copy-start.12 = (s32[32,2]{0,1:T(2,128)S(1)}, s32[32,2]{0,1:T(2,128)}, u32[]{:S(2)}) copy-start(s32[32,2]{0,1:T(2,128)} %param.38) | copy-start | bytes 772
  215.3 14.9 %copy-start.2 = (bf16[32,4096]{1,0:T(8,128)(2,1)}, bf16[32,4096]{1,0:T(8,128)(2,1)S(1)}, u32[]{:S(2)}) copy-start(bf16[32,4096]{1,0:T(8,128)(2,1)S(1)} %get-tuple-element.5) | copy-start | bytes 786436
  216.2 9.0 %all-to-all-start.4 = ((bf16[32,4,1024]{2,0,1:T(8,128)(2,1)}), bf16[32,4,1024]{2,0,1:T(8,128)(2,1)S(1)}, u32[]{:S(2)}, u32[]{:S(2)}) async-start(bf16[32,4,1024]{2,0,1:T(8,128)(2,1)} %bitcast.120), calls=%async_computation.8 | async-start | bytes 524288 | tf_op jit(solution)/shard_map/all_to_all | solution.py:122
  219.8 51.6 %reduce-scatter.17.cloned.1.call-start = ((), (), s32[]{:S(2)}) async-start(), calls=%async_computation.18 | async-start | bytes 655360 | tf_op jit(solution)/shard_map/reduce_scatter | solution.py:130
  245.0 11.9 %all-to-all-start.2 = ((bf16[4,22,4096]{2,1,0:T(8,128)(2,1)}), bf16[4,22,4096]{2,1,0:T(8,128)(2,1)S(1)}, u32[]{:S(2)}, u32[]{:S(2)}) async-start(bf16[4,22,4096]{2,1,0:T(8,128)(2,1)} %copy.67), calls=%async_computation.6 | async-start | bytes 1572864 | tf_op jit(solution)/shard_map/all_to_all | solution.py:156
  248.5 33.9 %reduce-scatter.15.cloned.1.call-start = ((), (), s32[]{:S(2)}) async-start(), calls=%async_computation.17 | async-start | bytes 655360 | tf_op jit(solution)/shard_map/reduce_scatter | solution.py:124
  259.9 10.7 %copy-start.10 = (f32[32,2]{0,1:T(2,128)S(1)}, f32[32,2]{0,1:T(2,128)}, u32[]{:S(2)}) copy-start(f32[32,2]{0,1:T(2,128)} %param.39) | copy-start | bytes 772
  259.9 11.4 %copy-start.9 = (bf16[4096]{0:T(1024)(128)(2,1)S(1)}, bf16[4096]{0:T(1024)(128)(2,1)}, u32[]{:S(2)}) copy-start(bf16[4096]{0:T(1024)(128)(2,1)} %param.37) | copy-start | bytes 24580
  266.3 28.8 %all-to-all-start.3 = ((f32[4,22,4096]{2,1,0:T(8,128)}), f32[4,22,4096]{2,1,0:T(8,128)}, u32[]{:S(2)}, u32[]{:S(2)}) async-start(f32[4,22,4096]{2,1,0:T(8,128)} %fusion), calls=%async_computation.7 | async-start | bytes 3145728 | tf_op jit(solution)/shard_map/all_to_all | solution.py:166
  295.1 14.7 %all-to-all-start.5 = ((f32[4,32,1024]{2,1,0:T(8,128)}), f32[4,32,1024]{2,1,0:T(8,128)}, u32[]{:S(2)}, u32[]{:S(2)}) async-start(f32[4,32,1024]{2,1,0:T(8,128)} %bitcast.30), calls=%async_computation.11 | async-start | bytes 1048576 | tf_op jit(solution)/shard_map/all_to_all | solution.py:143
  299.2 74.5 %all-reduce.5.cloned.1.call-start = ((), (), s32[]{:S(2)}) async-start(), calls=%async_computation.19 | async-start | bytes 1048576 | tf_op jit(solution)/shard_map/psum | solution.py:170
  304.9 68.8 %copy-start.3 = (bf16[32,4096]{1,0:T(8,128)(2,1)S(1)}, bf16[32,4096]{1,0:T(8,128)(2,1)}, u32[]{:S(2)}) copy-start(bf16[32,4096]{1,0:T(8,128)(2,1)} %copy-done.2) | copy-start | bytes 786436
Sparse Core Ops, SparseCore 0:
  22.9 24.2 reduce-scatter.8
  49.9 24.1 reduce-scatter.10
  77.4 24.1 reduce-scatter.6
  104.2 24.1 reduce-scatter.12
  158.1 55.9 all-reduce.2
  226.6 23.4 reduce-scatter.16
  252.9 29.3 reduce-scatter.14
  312.9 60.7 all-reduce.4
where the time goes:
time: 384 us; the launch traced here: 382 us
  waiting for transfers between devices  238 us (62%)
  local copies, waits for them, and re-layouts  33.2 us (9%)
  matrix products  30.9 us (8%)
  blocking collectives  26.7 us (7%)
  starting transfers between devices  21.1 us (5%)
  other arithmetic  17.9 us (5%)
  between operations  14.4 us (4%)
    psum x1, waiting for transfers between devices, on_device(): total_ffn = lax.psum(expert_rows + branch_share[:, None] * dense_back, 'tp')  60.9 us
    psum x1, waiting for transfers between devices, on_device(): mixer_out = lax.psum(mix_back, 'tp')  56.1 us
    reduce_scatter x1, waiting for transfers between devices, on_device(): lax.psum_scatter(part_k, 'ep', scatter_dimension=0, tiled=True)  26.1 us
    reduce_scatter x1, waiting for transfers between devices, on_device(): lax.psum_scatter(part_o, 'ep', scatter_dimension=0, tiled=True)  25.9 us
    reduce_scatter x1, waiting for transfers between devices, on_device(): lax.psum_scatter(part_v, 'ep', scatter_dimension=0, tiled=True)  25.9 us
    reduce_scatter x1, waiting for transfers between devices, on_device(): lax.psum_scatter(part_q, 'ep', scatter_dimension=0, tiled=True)  17.2 us
    scatter x2, local copies, waits for them, and re-layouts, on_device(): outbound = jnp.zeros((experts_all, capacity, model_width), jnp.bfloat16)....  14.5 us
    reduce_scatter x1, waiting for transfers between devices, on_device(): lax.psum_scatter(jnp.dot(dense_spread, dense_gate, preferred_element_type...  11 us
  transfers between devices with their start and end apart: 13, of which 10 were waited for; matrix products, arithmetic and copies ran while one was open for 15% of the time, Pallas kernels for 0%

commit v1 on v0

v1 whole, which is shorter than its diff:
```python
import functools

import jax
import jax.numpy as jnp
from jax import lax
from jax.experimental import pallas as pl
from jax.experimental.pallas import tpu as pltpu
from jax.sharding import PartitionSpec as P

EPS = 1e-06
F32 = jnp.float32
BF16 = jnp.bfloat16
MESH = pl.DeviceIdType.MESH


def remote(src, dst, sems, phase, k, peer):
    return pltpu.make_async_remote_copy(
        src_ref=src,
        dst_ref=dst,
        send_sem=sems[0].at[phase, k],
        recv_sem=sems[1].at[phase, k],
        device_id=peer,
        device_id_type=MESH,
    )


def around(n, me, make):
    copies = [make(k, lax.rem(me + k, n)) for k in range(1, n)]
    for copy in copies:
        copy.start()
    return copies


def finish(copies):
    for copy in copies:
        copy.wait()


def project_kernel(
    n_ep, n_tp,
    tokens, gain, w_q, w_k, w_v, w_o, w_in, w_fg, bias,
    proj, gates, spread,
    arrived, weights, gate_w, outgoing, incoming, send_sem, recv_sem, load_sem,
):
    e, t = lax.axis_index("ep"), lax.axis_index("tp")
    seqs, width = tokens.shape
    block = width // n_ep
    cols = w_q.shape[1]
    heads_all = bias.shape[1]
    heads = heads_all // n_tp
    sems = (send_sem, recv_sem)
    barrier = pltpu.get_barrier_semaphore()
    for k in range(1, n_ep):
        pl.semaphore_signal(
            barrier, inc=1, device_id={"ep": lax.rem(e + k, n_ep)}, device_id_type=MESH
        )
    loads = [
        pltpu.make_async_copy(src, dst, load_sem.at[i])
        for i, (src, dst) in enumerate(
            [(w_in, gate_w.at[0]), (w_fg, gate_w.at[1])]
            + [(w, weights.at[j]) for j, w in enumerate((w_q, w_k, w_v, w_o))]
        )
    ]
    for load in loads:
        load.start()
    pl.semaphore_wait(barrier, n_ep - 1)

    def columns(index):
        return pl.ds(pl.multiple_of(index * block, block), block)

    copies = around(
        n_ep, e,
        lambda k, p: remote(tokens.at[:, columns(p)], arrived.at[e], sems, 0, k, {"ep": p}),
    )
    wide = tokens[...].astype(F32)
    scale = lax.rsqrt(jnp.mean(wide * wide, axis=1, keepdims=True) + EPS)
    normed = (wide * scale * gain[...]).astype(BF16)
    loads[0].wait()
    loads[1].wait()
    gate_in = jnp.dot(normed, gate_w[0], preferred_element_type=F32)
    gate_fg = jnp.dot(normed, gate_w[1], preferred_element_type=F32) + bias[...]
    lane = lax.broadcasted_iota(jnp.int32, gate_in.shape, 1)
    for h in range(heads):
        mine = lane == t * heads + h
        gates[:, h : h + 1] = jnp.sum(jnp.where(mine, gate_in, 0.0), axis=1, keepdims=True)
        gates[:, heads + h : heads + h + 1] = jnp.sum(
            jnp.where(mine, gate_fg, 0.0), axis=1, keepdims=True
        )
    spread[e] = tokens[:, columns(e)]
    finish(copies)
    for k in range(1, n_ep):
        p = lax.rem(e + k, n_ep)
        spread[p] = arrived[p]
    scaled = spread[...].astype(F32).reshape(n_ep * seqs, block) * gain[:, columns(e)]
    scaled = scaled.astype(BF16)
    for j in range(4):
        loads[2 + j].wait()
        part = jnp.dot(scaled, weights[j], preferred_element_type=F32)
        outgoing[:, :, j * cols : (j + 1) * cols] = part.reshape(n_ep, seqs, cols).astype(BF16)
    finish(
        around(
            n_ep, e,
            lambda k, p: remote(outgoing.at[p], incoming.at[e], sems, 1, k, {"ep": p}),
        )
    )
    total = outgoing[e].astype(F32)
    for k in range(1, n_ep):
        total = total + incoming[lax.rem(e + k, n_ep)].astype(F32)
    proj[...] = total * scale


def cell_kernel(proj, gates, matrix, norm, top, mixed, new_matrix, new_norm, new_top):
    rows, heads, size, _ = matrix.shape
    gate_in = gates[:, :heads]
    gate_fg = gates[:, heads:]
    log_keep = jnp.minimum(gate_fg, 0.0) - jnp.log1p(jnp.exp(-jnp.abs(gate_fg)))
    highest = jnp.maximum(log_keep + top[...], gate_in)
    new_top[...] = highest
    keep = jnp.exp(log_keep + top[...] - highest)
    write = jnp.exp(gate_in - highest)
    width = heads * size
    for h in range(heads):
        at = h * size
        q = proj[:, at : at + size]
        key = proj[:, width + at : width + at + size] * (size ** (-0.5))
        val = proj[:, 2 * width + at : 2 * width + at + size]
        gate = proj[:, 3 * width + at : 3 * width + at + size]
        keep_h = keep[:, h : h + 1]
        added = write[:, h : h + 1] * key
        normal = keep_h * norm[:, h, :] + added
        new_norm[:, h, :] = normal
        denom = jnp.maximum(jnp.abs(jnp.sum(q * normal, axis=1, keepdims=True)), 1.0)
        q_t = q.T
        added_t = added.T
        numer = []
        for b in range(rows):
            fresh = keep_h[b : b + 1] * matrix[b, h] + added_t[:, b : b + 1] * val[b : b + 1]
            new_matrix[b, h] = fresh
            numer.append(jnp.sum(q_t[:, b : b + 1] * fresh, axis=0, keepdims=True))
        cell = jnp.concatenate(numer, axis=0) / denom
        mixed[:, at : at + size] = cell / (1.0 + jnp.exp(-gate))


def sigmoid(x):
    return 1.0 / (1.0 + jnp.exp(-x))


def ffn_kernel(
    n_ep, n_tp,
    mixed, spread, gain, branch, routes, route_weight,
    w_proj, d_gate, d_up, e_gate, e_up, d_down, e_down,
    out,
    v_proj, v_dgate, v_dup, v_egate, v_eup, v_ddown, v_edown,
    heads_all, shares, part, part_in, full, dense_part, dense_in, dense_hid,
    scale_ref, dense_out, halves, half_in, summed, summed_in, strips, strips_in, pieces,
    send_sem, recv_sem, load_sem,
):
    e, t = lax.axis_index("ep"), lax.axis_index("tp")
    core = lax.rem(t, 2)
    z = lax.div(t, 2)
    n_z = n_tp // 2
    seqs = mixed.shape[0]
    rows = n_ep * seqs
    chunk, block = spread.shape[1], spread.shape[2]
    width = n_ep * block
    hidden = d_gate.shape[1]
    local = e_gate.shape[0]
    sems = (send_sem, recv_sem)
    sibling = {"tp": t + 1 - 2 * core}
    half_t = n_tp // 2
    strip = width // n_tp

    barrier = pltpu.get_barrier_semaphore()
    for k in range(1, n_ep):
        pl.semaphore_signal(
            barrier, inc=1, device_id={"ep": lax.rem(e + k, n_ep)}, device_id_type=MESH
        )
    for k in range(1, n_tp):
        pl.semaphore_signal(
            barrier, inc=1, device_id={"tp": lax.rem(t + k, n_tp)}, device_id_type=MESH
        )
    loads = [
        pltpu.make_async_copy(src, dst, load_sem.at[i])
        for i, (src, dst) in enumerate(
            [(w_proj, v_proj), (d_gate, v_dgate), (d_up, v_dup), (e_gate, v_egate),
             (e_up, v_eup), (d_down, v_ddown), (e_down, v_edown)]
        )
    ]
    for load in loads:
        load.start()

    heads_all[e] = mixed[...].astype(BF16)
    weight = route_weight[...]
    share = weight / jnp.sum(weight, axis=1, keepdims=True)
    lane = lax.broadcasted_iota(jnp.int32, (seqs, shares.shape[2]), 1)
    table = jnp.zeros((seqs, shares.shape[2]), F32)
    for k in range(routes.shape[1]):
        table = table + jnp.where(lane == routes[:, k : k + 1], share[:, k : k + 1], 0.0)
    shares[e] = table
    pl.semaphore_wait(barrier, n_ep + n_tp - 2)

    copies = around(
        n_ep, e,
        lambda k, p: remote(heads_all.at[e], heads_all.at[e], sems, 0, k, {"ep": p}),
    )
    share_copies = around(
        n_ep, e, lambda k, p: remote(shares.at[e], shares.at[e], sems, 1, k, {"ep": p})
    )
    loads[0].wait()
    finish(copies)
    cols = heads_all.shape[2]
    mixer = jnp.dot(
        heads_all[...].reshape(rows, cols), v_proj[...], preferred_element_type=F32
    )
    part[...] = mixer.reshape(n_tp, chunk, block).astype(BF16)
    finish(
        around(
            n_tp, t, lambda k, p: remote(part.at[p], part_in.at[t], sems, 2, k, {"tp": p})
        )
    )
    total = part[t].astype(F32)
    for k in range(1, n_tp):
        total = total + part_in[lax.rem(t + k, n_tp)].astype(F32)
    full[e, t] = (spread[t].astype(F32) + total).astype(BF16)
    finish(
        around(
            n_tp, t,
            lambda k, p: remote(full.at[e, t], full.at[e, t], sems, 3, k, {"tp": p}),
        )
    )

    half = pl.ds(core * half_t, half_t)
    copies = around(
        n_ep, e,
        lambda k, p: remote(full.at[e, half], full.at[e, half], sems, 4, k, {"ep": p}),
    )
    own_gain = gain[:, pl.ds(pl.multiple_of(e * block, block), block)]
    own = (full[e].astype(F32).reshape(rows, block) * own_gain).astype(BF16)
    for i in range(2):
        loads[1 + i].wait()
        value = jnp.dot(own, (v_dgate, v_dup)[i][...], preferred_element_type=F32)
        dense_part[:, :, i * hidden : (i + 1) * hidden] = value.reshape(
            n_ep, seqs, hidden
        ).astype(BF16)
    dense_copies = around(
        n_ep, e,
        lambda k, p: remote(dense_part.at[p], dense_in.at[e], sems, 5, k, {"ep": p}),
    )
    passed = []
    for k in range(1, n_ep):
        copies[k - 1].wait_recv()
        origin = lax.rem(e + n_ep - k, n_ep)
        copy = remote(full.at[origin, half], full.at[origin, half], sems, 6, k, sibling)
        copy.start()
        passed.append(copy)
    for copy in copies:
        copy.wait_send()
    finish(passed)

    squares = jnp.zeros((rows, 1), F32)
    logit = jnp.zeros((rows, 1), F32)
    for j in range(n_ep):
        span = slice(j * block, (j + 1) * block)
        x = full[j].astype(F32).reshape(rows, block)
        squares = squares + jnp.sum(x * x, axis=1, keepdims=True)
        scaled = (x * gain[:, span]).astype(BF16).astype(F32)
        logit = logit + jnp.sum(scaled * branch[:, span].astype(F32), axis=1, keepdims=True)
    scale = lax.rsqrt(squares / width + EPS)
    branch_share = sigmoid(logit * scale)
    scale_ref[...] = jnp.broadcast_to(scale, scale_ref.shape)

    finish(dense_copies)
    total = dense_part[e].astype(F32)
    for k in range(1, n_ep):
        total = total + dense_in[lax.rem(e + k, n_ep)].astype(F32)
    total = total * scale_ref[pl.ds(pl.multiple_of(e * seqs, seqs), seqs), 0:1]
    gate = total[:, :hidden]
    dense_hid[e] = (gate * sigmoid(gate) * total[:, hidden:]).astype(BF16)
    copies = around(
        n_ep, e,
        lambda k, p: remote(dense_hid.at[e], dense_hid.at[e], sems, 7, k, {"ep": p}),
    )

    loads[3].wait()
    loads[4].wait()
    finish(share_copies)
    table = shares[...].reshape(rows, shares.shape[2])
    lane = lax.broadcasted_iota(jnp.int32, table.shape, 1)
    expert_hid, expert_share = [], []
    for l in range(local):
        gate = up = None
        for j in range(n_ep):
            span = slice(j * block, (j + 1) * block)
            x = (full[j].astype(F32).reshape(rows, block) * gain[:, span]).astype(BF16)
            g = jnp.dot(x, v_egate[l, span, :], preferred_element_type=F32)
            u = jnp.dot(x, v_eup[l, span, :], preferred_element_type=F32)
            gate = g if gate is None else gate + g
            up = u if up is None else up + u
        gate, up = gate * scale, up * scale
        expert_hid.append((gate * sigmoid(gate) * up).astype(BF16))
        expert_share.append(
            jnp.sum(jnp.where(lane == e * local + l, table, 0.0), axis=1, keepdims=True)
        )
    finish(copies)
    loads[5].wait()
    dense_out[...] = branch_share * jnp.dot(
        dense_hid[...].reshape(rows, hidden), v_ddown[...], preferred_element_type=F32
    )
    loads[6].wait()
    for j in range(n_ep):
        value = jnp.where(e == j, dense_out[...], 0.0)
        for l in range(local):
            value = value + expert_share[l] * jnp.dot(
                expert_hid[l],
                v_edown[l, :, j * block : (j + 1) * block],
                preferred_element_type=F32,
            )
        side, at = (j * block) // (width // 2), (j * block) % (width // 2)
        halves[side, :, :, at : at + block] = value.reshape(n_ep, seqs, block).astype(BF16)

    finish_pair = remote(halves.at[1 - core], half_in, sems, 8, 0, sibling)
    finish_pair.start()
    finish_pair.wait()
    summed[...] = (halves[core].astype(F32) + half_in[...].astype(F32)).astype(BF16)
    finish(
        around(
            n_ep, e, lambda k, p: remote(summed.at[p], summed_in.at[e], sems, 9, k, {"ep": p})
        )
    )
    total = summed[e].astype(F32)
    for k in range(1, n_ep):
        total = total + summed_in[lax.rem(e + k, n_ep)].astype(F32)
    for i in range(n_z):
        strips[i] = total[:, i * strip : (i + 1) * strip].astype(BF16)
    finish(
        around(
            n_z, z,
            lambda k, p: remote(
                strips.at[p], strips_in.at[z], sems, 10, k, {"tp": 2 * p + core}
            ),
        )
    )
    total = strips[z].astype(F32)
    for k in range(1, n_z):
        total = total + strips_in[lax.rem(z + k, n_z)].astype(F32)
    place = core * n_z + z
    per_block = block // strip
    held = full[
        lax.div(place, per_block),
        pl.ds(e * (seqs // chunk), seqs // chunk),
        :,
        pl.ds(pl.multiple_of(lax.rem(place, per_block) * strip, strip), strip),
    ]
    pieces[place] = (held.astype(F32).reshape(seqs, strip) + total).astype(BF16)
    finish(
        around(
            n_z, z,
            lambda k, p: remote(
                pieces.at[place], pieces.at[place], sems, 11, k, {"tp": 2 * p + core}
            ),
        )
    )
    side = pl.ds(core * n_z, n_z)
    copy = remote(pieces.at[side], pieces.at[side], sems, 12, 0, sibling)
    copy.start()
    copy.wait()
    for i in range(n_tp):
        out[:, i * strip : (i + 1) * strip] = pieces[i]


def on_device(
    n_ep, n_tp,
    tokens, state_matrix, state_norm, state_max, mixer_gain, w_query, w_key, w_value, w_outgate,
    w_ingate, w_forget, forget_bias, w_proj, ffn_gain, w_branch, routes, route_weight,
    expert_gate, expert_up, expert_down, dense_gate, dense_up, dense_down,
):
    seqs, width = tokens.shape
    heads, size = state_matrix.shape[1], state_matrix.shape[2]
    block, cols = w_query.shape
    heads_all = w_ingate.shape[1]
    vmem = pl.BlockSpec(memory_space=pltpu.VMEM)
    any_ = pl.BlockSpec(memory_space=pl.ANY)
    limit = 60 * 1024 * 1024

    proj, gates, spread = pl.pallas_call(
        functools.partial(project_kernel, n_ep, n_tp),
        out_shape=(
            jax.ShapeDtypeStruct((seqs, 4 * cols), F32),
            jax.ShapeDtypeStruct((seqs, 2 * heads), F32),
            jax.ShapeDtypeStruct((n_ep, seqs, block), BF16),
        ),
        in_specs=[vmem, vmem, any_, any_, any_, any_, any_, any_, vmem],
        out_specs=(vmem, vmem, vmem),
        scratch_shapes=[
            pltpu.VMEM((n_ep, seqs, block), BF16),
            pltpu.VMEM((4, block, cols), BF16),
            pltpu.VMEM((2, width, heads_all), BF16),
            pltpu.VMEM((n_ep, seqs, 4 * cols), BF16),
            pltpu.VMEM((n_ep, seqs, 4 * cols), BF16),
            pltpu.SemaphoreType.DMA((2, n_ep)),
            pltpu.SemaphoreType.DMA((2, n_ep)),
            pltpu.SemaphoreType.DMA((6,)),
        ],
        compiler_params=pltpu.CompilerParams(
            collective_id=0, has_side_effects=True, vmem_limit_bytes=limit
        ),
        name="project",
    )(
        tokens, mixer_gain.reshape(1, width), w_query, w_key, w_value, w_outgate,
        w_ingate, w_forget, forget_bias.reshape(1, heads_all),
    )

    group = 8
    mixed, new_matrix, new_norm, new_max = pl.pallas_call(
        cell_kernel,
        grid=(seqs // group,),
        out_shape=(
            jax.ShapeDtypeStruct((seqs, cols), F32),
            jax.ShapeDtypeStruct(state_matrix.shape, F32),
            jax.ShapeDtypeStruct(state_norm.shape, F32),
            jax.ShapeDtypeStruct(state_max.shape, F32),
        ),
        in_specs=[
            pl.BlockSpec((group, 4 * cols), lambda i: (i, 0)),
            pl.BlockSpec((group, 2 * heads), lambda i: (i, 0)),
            pl.BlockSpec((group, heads, size, size), lambda i: (i, 0, 0, 0)),
            pl.BlockSpec((group, heads, size), lambda i: (i, 0, 0)),
            pl.BlockSpec((group, heads), lambda i: (i, 0)),
        ],
        out_specs=(
            pl.BlockSpec((group, cols), lambda i: (i, 0)),
            pl.BlockSpec((group, heads, size, size), lambda i: (i, 0, 0, 0)),
            pl.BlockSpec((group, heads, size), lambda i: (i, 0, 0)),
            pl.BlockSpec((group, heads), lambda i: (i, 0)),
        ),
        name="cell",
    )(proj, gates, state_matrix, state_norm, state_max)

    rows = n_ep * seqs
    chunk = rows // n_tp
    hidden = dense_gate.shape[1]
    strip = width // n_tp
    lanes = -(-(n_ep * expert_gate.shape[0]) // 128) * 128
    phases, most = 13, max(n_ep, n_tp)
    layer_out = pl.pallas_call(
        functools.partial(ffn_kernel, n_ep, n_tp),
        out_shape=jax.ShapeDtypeStruct((seqs, width), BF16),
        in_specs=[vmem] * 6 + [any_] * 7,
        out_specs=vmem,
        scratch_shapes=[
            pltpu.VMEM(w.shape, BF16)
            for w in (w_proj, dense_gate, dense_up, expert_gate, expert_up, dense_down, expert_down)
        ]
        + [
            pltpu.VMEM((n_ep, seqs, cols), BF16),
            pltpu.VMEM((n_ep, seqs, lanes), F32),
            pltpu.VMEM((n_tp, chunk, block), BF16),
            pltpu.VMEM((n_tp, chunk, block), BF16),
            pltpu.VMEM((n_ep, n_tp, chunk, block), BF16),
            pltpu.VMEM((n_ep, seqs, 2 * hidden), BF16),
            pltpu.VMEM((n_ep, seqs, 2 * hidden), BF16),
            pltpu.VMEM((n_ep, seqs, hidden), BF16),
            pltpu.VMEM((rows, 128), F32),
            pltpu.VMEM((rows, block), F32),
            pltpu.VMEM((2, n_ep, seqs, width // 2), BF16),
            pltpu.VMEM((n_ep, seqs, width // 2), BF16),
            pltpu.VMEM((n_ep, seqs, width // 2), BF16),
            pltpu.VMEM((n_ep, seqs, width // 2), BF16),
            pltpu.VMEM((n_tp // 2, seqs, strip), BF16),
            pltpu.VMEM((n_tp // 2, seqs, strip), BF16),
            pltpu.VMEM((n_tp, seqs, strip), BF16),
            pltpu.SemaphoreType.DMA((phases, most)),
            pltpu.SemaphoreType.DMA((phases, most)),
            pltpu.SemaphoreType.DMA((7,)),
        ],
        compiler_params=pltpu.CompilerParams(
            collective_id=1, has_side_effects=True, vmem_limit_bytes=limit
        ),
        name="feedforward",
    )(
        mixed, spread.reshape(n_tp, chunk, block), ffn_gain.reshape(1, width),
        w_branch.reshape(1, width), routes, route_weight,
        w_proj, dense_gate, dense_up, expert_gate, expert_up, dense_down, expert_down,
    )
    return (layer_out, new_matrix, new_norm, new_max)


def solution(mesh):
    in_specs = (
        P("ep", None),
        P("ep", "tp", None, None),
        P("ep", "tp", None),
        P("ep", "tp"),
        P(),
        P("ep", "tp"),
        P("ep", "tp"),
        P("ep", "tp"),
        P("ep", "tp"),
        P(),
        P(),
        P(),
        P("tp", "ep"),
        P(),
        P(),
        P("ep", None),
        P("ep", None),
        P("ep", None, "tp"),
        P("ep", None, "tp"),
        P("ep", "tp", None),
        P("ep", "tp"),
        P("ep", "tp"),
        P("tp", "ep"),
    )
    out_specs = (P("ep", None), P("ep", "tp", None, None), P("ep", "tp", None), P("ep", "tp"))
    step = functools.partial(on_device, mesh.shape["ep"], mesh.shape["tp"])
    return jax.shard_map(step, mesh=mesh, in_specs=in_specs, out_specs=out_specs, check_vma=False)
```

time: 384 us -> 99 us (0.26)
  waiting for transfers between devices: 238 us -> 0 us
  Pallas kernels: 0 us -> 85.8 us
  matrix products: 30.9 us -> 0 us
  blocking collectives: 26.7 us -> 0 us
  local copies, waits for them, and re-layouts: 33.2 us -> 12.1 us
  starting transfers between devices: 21.1 us -> 0 us
  other arithmetic: 17.9 us -> 0 us
  between operations: 14.4 us -> 0.66 us
    psum x2 -> x0, waiting for transfers between devices: 117 us -> none  [the longest x1 60.9 us: on_device(): total_ffn = lax.psum(expert_rows + branch_share[:, None] * dense_back, 'tp')]
    reduce_scatter x6 -> x0, waiting for transfers between devices: 106 us -> none  [the longest x1 26.1 us: on_device(): lax.psum_scatter(part_k, 'ep', scatter_dimension=0, tiled=True)]
    pallas_call x0 -> x3, Pallas kernels: none -> 85.8 us  [the longest x1 62.3 us: on_device(): pl.pallas_call(functools.partial(ffn_kernel, n_ep, n_tp), out_shape=jax.S...]
    dot_general x14 -> x0, matrix products: 30.9 us -> none  [the longest x1 6.32 us: on_device(): jnp.einsum('secf,efd->secd', hidden, expert_down, preferred_element_type=...]
    all_to_all x5 -> x0, starting transfers between devices: 20.8 us -> none  [the longest x1 5.19 us: on_device(): lax.all_to_all(normed, 'ep', split_axis=1, concat_axis=0, tiled=True)]
    all_gather x2 -> x0, blocking collectives: 17.1 us -> none  [the longest x1 8.89 us: on_device(): lax.all_gather(dense_hidden, 'ep', axis=0, tiled=True)]
    all_to_all x5 -> x0, waiting for transfers between devices: 14.8 us -> none  [the longest x1 5.46 us: on_device(): lax.all_to_all(outbound, 'ep', split_axis=0, concat_axis=0, tiled=True)]
    scatter x2 -> x0, local copies, waits for them, and re-layouts: 14.5 us -> none  [on_device(): outbound = jnp.zeros((experts_all, capacity, model_width), jnp.bfloat16)....]
  transfers between devices with their start and end apart: 13 -> 0, of which waited for: 10 -> 0; matrix products, arithmetic and copies ran while one was open for 15% -> 0% of each run, Pallas kernels for 0% -> 0%
where the time goes in v1:
time: 99 us; the launch traced here: 98.6 us
  Pallas kernels  85.8 us (87%)
  local copies, waits for them, and re-layouts  12.1 us (12%)
    pallas_call x1, Pallas kernels, on_device(): pl.pallas_call(functools.partial(ffn_kernel, n_ep, n_tp), out_shape=jax.S...  62.3 us
    pallas_call x1, Pallas kernels, on_device(): pl.pallas_call(functools.partial(project_kernel, n_ep, n_tp), out_shape=(...  15.6 us
    unnamed x9, local copies, waits for them, and re-layouts  10.8 us
    pallas_call x1, Pallas kernels, on_device(): pl.pallas_call(cell_kernel, grid=(seqs // group,), out_shape=(jax.ShapeDt...  7.9 us

profile of v1, /device:TPU:0, one launch (start us, length us, event | category | flops | bytes accessed | tf_op | source)
XLA Modules:
  0.0 98.6 jit_solution(1117986227603665584)
XLA Ops:
  0.6 1.4 %copy.29.top = f32[32,2]{1,0:T(8,128)} copy(f32[32,2]{0,1:T(2,128)} %param.26) | data formatting | bytes 512 | tf_op args[3]
  2.0 1.3 %reshape.27.branch = bf16[1,4096]{1,0:T(2,128)(2,1)} reshape(bf16[4096]{0:T(1024)(128)(2,1)} %param.37) | data formatting | bytes 16384 | tf_op jit(solution)/shard_map/reshape | solution.py:482
  3.3 1.4 %copy.30.routes = s32[32,2]{1,0:T(8,128)} copy(s32[32,2]{0,1:T(2,128)} %param.38) | data formatting | bytes 512 | tf_op args[15]
  4.7 1.4 %copy.31.route_weight = f32[32,2]{1,0:T(8,128)} copy(f32[32,2]{0,1:T(2,128)} %param.39) | data formatting | bytes 512 | tf_op args[16]
  6.0 2.2 %copy.27.w_in = bf16[4096,16]{1,0:T(8,128)(2,1)} copy(bf16[4096,16]{0,1:T(8,128)(2,1)} %param.32) | data formatting | bytes 262144 | tf_op args[9]
  8.2 2.2 %copy.28.w_fg = bf16[4096,16]{1,0:T(8,128)(2,1)} copy(bf16[4096,16]{0,1:T(8,128)(2,1)} %param.33) | data formatting | bytes 262144 | tf_op args[10]
  10.5 15.6 %project.1 = (f32[32,1024]{1,0:T(8,128)}, f32[32,4]{1,0:T(8,128)}, bf16[4,32,1024]{2,1,0:T(8,128)(2,1)}) custom-call(bf16[32,4096]{1,0:T(8,128)(2,1)} %tokens.1, f32[1,4096]{1,0:T(1,128)} %bitcast.5, bf16[1024,256]{1,0:T(8,128)(2,1)} %w_q.1, bf16[1024,256]{1,0:T(8,128)(2,1)} %w_k.1, bf16[1024,256]{1,0:T(8,128)(2,1)} %w_v.1, bf16[1024,256]{1,0:T(8,128)(2,1)} %w_o.1, ...), custom_call_target="tpu_custom_call" | custom-call | tf_op jit(solution)/shard_map/project/pallas_call | solution.py:385
  26.0 7.9 %cell.1 = (f32[32,256]{1,0:T(8,128)}, f32[32,2,128,128]{3,2,1,0:T(8,128)}, f32[32,2,128]{2,1,0:T(2,128)}, f32[32,2]{1,0:T(8,128)}) custom-call(f32[32,1024]{1,0:T(8,128)} %get-tuple-element.11.proj, f32[32,4]{1,0:T(8,128)} %get-tuple-element.12.gates, f32[32,2,128,128]{3,2,1,0:T(8,128)} %matrix.1, f32[32,2,128]{2,1,0:T(2,128)} %norm.1, f32[32,2]{1,0:T(8,128)} %copy.29.top), custom_call_target="tpu_custom_call" | custom-call | tf_op jit(solution)/shard_map/cell/pallas_call | solution.py:414
  33.9 0.0 copy-start
  33.9 62.3 %feedforward.1 = bf16[32,4096]{1,0:T(8,128)(2,1)} custom-call(f32[32,256]{1,0:T(8,128)} %get-tuple-element.13.mixed, bf16[8,16,1024]{2,1,0:T(8,128)(2,1)} %bitcast.4, f32[1,4096]{1,0:T(1,128)} %bitcast.6, bf16[1,4096]{1,0:T(2,128)(2,1)} %reshape.27.branch, s32[32,2]{1,0:T(8,128)} %copy.30.routes, f32[32,2]{1,0:T(8,128)} %copy.31.route_weight, ...), custom_call_target="tpu_custom_call" | custom-call | tf_op jit(solution)/shard_map/feedforward/pallas_call | solution.py:445
  96.2 0.0 copy-done
  96.3 0.6 copy.32
  96.9 1.7 %copy.34 = bf16[32,4096]{1,0:T(8,128)(2,1)} copy(bf16[32,4096]{1,0:T(8,128)(2,1)} %feedforward.1) | data formatting | bytes 524288
Async XLA Ops:
  33.9 62.3 %copy-start = (f32[32,2]{1,0:T(8,128)S(1)}, f32[32,2]{1,0:T(8,128)}, u32[]{:S(2)}) copy-start(f32[32,2]{1,0:T(8,128)} %get-tuple-element.21) | copy-start | bytes 772

commit v2 on v1

--- a/solution.py
+++ b/solution.py
@@ -36,10 +36,18 @@
         copy.wait()
 
 
+def column(row):
+    n = row.shape[1]
+    down = lax.broadcasted_iota(jnp.int32, (n, n), 0)
+    along = lax.broadcasted_iota(jnp.int32, (n, n), 1)
+    spread_row = jnp.broadcast_to(row, (n, n))
+    return jnp.sum(jnp.where(down == along, spread_row, 0.0), axis=1, keepdims=True)
+
+
 def project_kernel(
     n_ep, n_tp,
-    tokens, gain, w_q, w_k, w_v, w_o, w_in, w_fg, bias,
-    proj, gates, spread,
+    tokens, gain, w_q, w_k, w_v, w_o, w_in, w_fg, bias, top,
+    proj, gates, new_top, spread,
     arrived, weights, gate_w, outgoing, incoming, send_sem, recv_sem, load_sem,
 ):
     e, t = lax.axis_index("ep"), lax.axis_index("tp")
@@ -77,15 +85,22 @@
     normed = (wide * scale * gain[...]).astype(BF16)
     loads[0].wait()
     loads[1].wait()
-    gate_in = jnp.dot(normed, gate_w[0], preferred_element_type=F32)
-    gate_fg = jnp.dot(normed, gate_w[1], preferred_element_type=F32) + bias[...]
-    lane = lax.broadcasted_iota(jnp.int32, gate_in.shape, 1)
+    contract = (((1,), (1,)), ((), ()))
+    gate_in = lax.dot_general(gate_w[0], normed, contract, preferred_element_type=F32)
+    gate_fg = lax.dot_general(gate_w[1], normed, contract, preferred_element_type=F32)
+    down = lax.broadcasted_iota(jnp.int32, gate_in.shape, 0)
+    along = lax.broadcasted_iota(jnp.int32, bias.shape, 1)
     for h in range(heads):
-        mine = lane == t * heads + h
-        gates[:, h : h + 1] = jnp.sum(jnp.where(mine, gate_in, 0.0), axis=1, keepdims=True)
-        gates[:, heads + h : heads + h + 1] = jnp.sum(
-            jnp.where(mine, gate_fg, 0.0), axis=1, keepdims=True
-        )
+        head = t * heads + h
+        shift = jnp.sum(jnp.where(along == head, bias[...], 0.0), axis=1, keepdims=True)
+        entry = jnp.sum(jnp.where(down == head, gate_in, 0.0), axis=0, keepdims=True)
+        forget = jnp.sum(jnp.where(down == head, gate_fg, 0.0), axis=0, keepdims=True) + shift
+        log_keep = jnp.minimum(forget, 0.0) - jnp.log1p(jnp.exp(-jnp.abs(forget)))
+        kept = log_keep + top[h : h + 1, :]
+        highest = jnp.maximum(kept, entry)
+        new_top[h : h + 1, :] = highest
+        gates[:, h : h + 1] = column(jnp.exp(kept - highest))
+        gates[:, heads + h : heads + h + 1] = column(jnp.exp(entry - highest))
     spread[e] = tokens[:, columns(e)]
     finish(copies)
     for k in range(1, n_ep):
@@ -110,14 +125,10 @@
 
 
 def cell_kernel(proj, gates, matrix, norm, top, mixed, new_matrix, new_norm, new_top):
+    new_top[...] = top[...]
     rows, heads, size, _ = matrix.shape
-    gate_in = gates[:, :heads]
-    gate_fg = gates[:, heads:]
-    log_keep = jnp.minimum(gate_fg, 0.0) - jnp.log1p(jnp.exp(-jnp.abs(gate_fg)))
-    highest = jnp.maximum(log_keep + top[...], gate_in)
-    new_top[...] = highest
-    keep = jnp.exp(log_keep + top[...] - highest)
-    write = jnp.exp(gate_in - highest)
+    keep = gates[:, :heads]
+    write = gates[:, heads:]
     width = heads * size
     for h in range(heads):
         at = h * size
@@ -151,9 +162,9 @@
     w_proj, d_gate, d_up, e_gate, e_up, d_down, e_down,
     out,
     v_proj, v_dgate, v_dup, v_egate, v_eup, v_ddown, v_edown,
-    heads_all, shares, part, part_in, full, dense_part, dense_in, dense_hid,
-    scale_ref, dense_out, halves, half_in, summed, summed_in, strips, strips_in, pieces,
-    send_sem, recv_sem, load_sem,
+    heads_all, shares, part, part_in, part_sum, part_z, full, dense_part, dense_in, dense_hid,
+    scale_ref, halves, half_in, summed, summed_in, strips, strips_in, pieces,
+    send_sem, recv_sem, ep_send, ep_recv, fw_send, fw_recv, rs_send, rs_recv, load_sem,
 ):
     e, t = lax.axis_index("ep"), lax.axis_index("tp")
     core = lax.rem(t, 2)
@@ -167,7 +178,6 @@
     local = e_gate.shape[0]
     sems = (send_sem, recv_sem)
     sibling = {"tp": t + 1 - 2 * core}
-    half_t = n_tp // 2
     strip = width // n_tp
 
     barrier = pltpu.get_barrier_semaphore()
@@ -175,10 +185,11 @@
         pl.semaphore_signal(
             barrier, inc=1, device_id={"ep": lax.rem(e + k, n_ep)}, device_id_type=MESH
         )
-    for k in range(1, n_tp):
+    for k in range(1, n_z):
         pl.semaphore_signal(
-            barrier, inc=1, device_id={"tp": lax.rem(t + k, n_tp)}, device_id_type=MESH
-        )
+            barrier, inc=1, device_id={"tp": lax.rem(t + 2 * k, n_tp)}, device_id_type=MESH
+        )
+    pl.semaphore_signal(barrier, inc=1, device_id=sibling, device_id_type=MESH)
     loads = [
         pltpu.make_async_copy(src, dst, load_sem.at[i])
         for i, (src, dst) in enumerate(
@@ -191,13 +202,15 @@
 
     heads_all[e] = mixed[...].astype(BF16)
     weight = route_weight[...]
-    share = weight / jnp.sum(weight, axis=1, keepdims=True)
+    share = weight / jnp.sum(weight, axis=0, keepdims=True)
+    named = routes[...].astype(F32)
     lane = lax.broadcasted_iota(jnp.int32, (seqs, shares.shape[2]), 1)
     table = jnp.zeros((seqs, shares.shape[2]), F32)
-    for k in range(routes.shape[1]):
-        table = table + jnp.where(lane == routes[:, k : k + 1], share[:, k : k + 1], 0.0)
+    for k in range(routes.shape[0]):
+        chosen = lane.astype(F32) == column(named[k : k + 1])
+        table = table + jnp.where(chosen, column(share[k : k + 1]), 0.0)
     shares[e] = table
-    pl.semaphore_wait(barrier, n_ep + n_tp - 2)
+    pl.semaphore_wait(barrier, n_ep + n_z - 1)
 
     copies = around(
         n_ep, e,
@@ -212,28 +225,43 @@
     mixer = jnp.dot(
         heads_all[...].reshape(rows, cols), v_proj[...], preferred_element_type=F32
     )
-    part[...] = mixer.reshape(n_tp, chunk, block).astype(BF16)
+    part[...] = mixer.reshape(2, n_z, chunk, block).astype(BF16)
+    copy = remote(part.at[1 - core], part_in, sems, 2, 0, sibling)
+    copy.start()
+    copy.wait()
+    part_sum[...] = (part[core].astype(F32) + part_in[...].astype(F32)).astype(BF16)
     finish(
         around(
-            n_tp, t, lambda k, p: remote(part.at[p], part_in.at[t], sems, 2, k, {"tp": p})
-        )
-    )
-    total = part[t].astype(F32)
-    for k in range(1, n_tp):
-        total = total + part_in[lax.rem(t + k, n_tp)].astype(F32)
-    full[e, t] = (spread[t].astype(F32) + total).astype(BF16)
-    finish(
-        around(
-            n_tp, t,
-            lambda k, p: remote(full.at[e, t], full.at[e, t], sems, 3, k, {"tp": p}),
-        )
-    )
-
-    half = pl.ds(core * half_t, half_t)
-    copies = around(
-        n_ep, e,
-        lambda k, p: remote(full.at[e, half], full.at[e, half], sems, 4, k, {"ep": p}),
-    )
+            n_z, z,
+            lambda k, p: remote(
+                part_sum.at[p], part_z.at[z], sems, 3, k, {"tp": 2 * p + core}
+            ),
+        )
+    )
+    total = part_sum[z].astype(F32)
+    for k in range(1, n_z):
+        total = total + part_z[lax.rem(z + k, n_z)].astype(F32)
+    place = core * n_z + z
+    full[e, place] = (spread[place].astype(F32) + total).astype(BF16)
+
+    def same(a, b, sem_pair, i, k, peer):
+        return remote(full.at[a, b], full.at[a, b], sem_pair, i, k, peer)
+
+    z_copies = around(
+        n_z, z, lambda k, p: same(e, place, sems, 4, k, {"tp": 2 * p + core})
+    )
+    ep_sems, fw_sems = (ep_send, ep_recv), (fw_send, fw_recv)
+    ep_copies, passed = [], []
+    for i in range(n_z):
+        spot = core * n_z + lax.rem(z + n_z - i, n_z)
+        if i > 0:
+            z_copies[i - 1].wait_recv()
+        passed.append(same(e, spot, fw_sems, i, 0, sibling))
+        passed[-1].start()
+        ep_copies.append(
+            around(n_ep, e, lambda k, p: same(e, spot, ep_sems, i, k, {"ep": p}))
+        )
+    finish(passed)
     own_gain = gain[:, pl.ds(pl.multiple_of(e * block, block), block)]
     own = (full[e].astype(F32).reshape(rows, block) * own_gain).astype(BF16)
     for i in range(2):
@@ -244,17 +272,20 @@
         ).astype(BF16)
     dense_copies = around(
         n_ep, e,
-        lambda k, p: remote(dense_part.at[p], dense_in.at[e], sems, 5, k, {"ep": p}),
+        lambda k, p: remote(dense_part.at[p], dense_in.at[e], sems, 6, k, {"ep": p}),
     )
     passed = []
-    for k in range(1, n_ep):
-        copies[k - 1].wait_recv()
-        origin = lax.rem(e + n_ep - k, n_ep)
-        copy = remote(full.at[origin, half], full.at[origin, half], sems, 6, k, sibling)
-        copy.start()
-        passed.append(copy)
-    for copy in copies:
+    for i in range(n_z):
+        spot = core * n_z + lax.rem(z + n_z - i, n_z)
+        for k in range(1, n_ep):
+            ep_copies[i][k - 1].wait_recv()
+            passed.append(same(lax.rem(e + n_ep - k, n_ep), spot, fw_sems, i, k, sibling))
+            passed[-1].start()
+    for copy in z_copies:
         copy.wait_send()
+    for group in ep_copies:
+        for copy in group:
+            copy.wait_send()
     finish(passed)
 
     squares = jnp.zeros((rows, 1), F32)
@@ -268,18 +299,6 @@
     scale = lax.rsqrt(squares / width + EPS)
     branch_share = sigmoid(logit * scale)
     scale_ref[...] = jnp.broadcast_to(scale, scale_ref.shape)
-
-    finish(dense_copies)
-    total = dense_part[e].astype(F32)
-    for k in range(1, n_ep):
-        total = total + dense_in[lax.rem(e + k, n_ep)].astype(F32)
-    total = total * scale_ref[pl.ds(pl.multiple_of(e * seqs, seqs), seqs), 0:1]
-    gate = total[:, :hidden]
-    dense_hid[e] = (gate * sigmoid(gate) * total[:, hidden:]).astype(BF16)
-    copies = around(
-        n_ep, e,
-        lambda k, p: remote(dense_hid.at[e], dense_hid.at[e], sems, 7, k, {"ep": p}),
-    )
 
     loads[3].wait()
     loads[4].wait()
@@ -301,49 +320,76 @@
         expert_share.append(
             jnp.sum(jnp.where(lane == e * local + l, table, 0.0), axis=1, keepdims=True)
         )
-    finish(copies)
-    loads[5].wait()
-    dense_out[...] = branch_share * jnp.dot(
-        dense_hid[...].reshape(rows, hidden), v_ddown[...], preferred_element_type=F32
-    )
+    finish(dense_copies)
+    total = dense_part[e].astype(F32)
+    for k in range(1, n_ep):
+        total = total + dense_in[lax.rem(e + k, n_ep)].astype(F32)
+    total = total * scale_ref[pl.ds(pl.multiple_of(e * seqs, seqs), seqs), 0:1]
+    gate = total[:, :hidden]
+    dense_hid[e] = (gate * sigmoid(gate) * total[:, hidden:]).astype(BF16)
+    copies = around(
+        n_ep, e,
+        lambda k, p: remote(dense_hid.at[e], dense_hid.at[e], sems, 7, k, {"ep": p}),
+    )
+
     loads[6].wait()
     for j in range(n_ep):
-        value = jnp.where(e == j, dense_out[...], 0.0)
+        value = None
         for l in range(local):
-            value = value + expert_share[l] * jnp.dot(
+            term = expert_share[l] * jnp.dot(
                 expert_hid[l],
                 v_edown[l, :, j * block : (j + 1) * block],
                 preferred_element_type=F32,
             )
+            value = term if value is None else value + term
         side, at = (j * block) // (width // 2), (j * block) % (width // 2)
         halves[side, :, :, at : at + block] = value.reshape(n_ep, seqs, block).astype(BF16)
-
-    finish_pair = remote(halves.at[1 - core], half_in, sems, 8, 0, sibling)
+    finish(copies)
+    loads[5].wait()
+    dense_out = branch_share * jnp.dot(
+        dense_hid[...].reshape(rows, hidden), v_ddown[...], preferred_element_type=F32
+    )
+    per_half = n_ep // 2
+    side = lax.div(e, per_half)
+    at = pl.ds(pl.multiple_of(lax.rem(e, per_half) * block, block), block)
+    halves[side, :, :, at] = (
+        halves[side, :, :, at].astype(F32) + dense_out.reshape(n_ep, seqs, block)
+    ).astype(BF16)
+
+    finish_pair = remote(halves.at[1 - core], half_in, sems, 5, 0, sibling)
     finish_pair.start()
     finish_pair.wait()
-    summed[...] = (halves[core].astype(F32) + half_in[...].astype(F32)).astype(BF16)
-    finish(
+    for i in range(n_z):
+        cut = slice(i * strip, (i + 1) * strip)
+        summed[i] = (
+            halves[core, :, :, cut].astype(F32) + half_in[:, :, cut].astype(F32)
+        ).astype(BF16)
+    rs_sems = (rs_send, rs_recv)
+    order = [lax.rem(z + i, n_z) for i in range(1, n_z + 1)]
+    scatter = [
         around(
-            n_ep, e, lambda k, p: remote(summed.at[p], summed_in.at[e], sems, 9, k, {"ep": p})
-        )
-    )
-    total = summed[e].astype(F32)
-    for k in range(1, n_ep):
-        total = total + summed_in[lax.rem(e + k, n_ep)].astype(F32)
-    for i in range(n_z):
-        strips[i] = total[:, i * strip : (i + 1) * strip].astype(BF16)
-    finish(
-        around(
-            n_z, z,
+            n_ep, e,
             lambda k, p: remote(
-                strips.at[p], strips_in.at[z], sems, 10, k, {"tp": 2 * p + core}
+                summed.at[q, p], summed_in.at[q, e], rs_sems, i, k, {"ep": p}
             ),
         )
-    )
-    total = strips[z].astype(F32)
+        for i, q in enumerate(order)
+    ]
+    z_copies = []
+    for i, q in enumerate(order):
+        finish(scatter[i])
+        total = summed[q, e].astype(F32)
+        for k in range(1, n_ep):
+            total = total + summed_in[q, lax.rem(e + k, n_ep)].astype(F32)
+        if i < n_z - 1:
+            strips[q] = total.astype(BF16)
+            z_copies.append(
+                remote(strips.at[q], strips_in.at[z], sems, 8, i + 1, {"tp": 2 * q + core})
+            )
+            z_copies[-1].start()
+    finish(z_copies)
     for k in range(1, n_z):
         total = total + strips_in[lax.rem(z + k, n_z)].astype(F32)
-    place = core * n_z + z
     per_block = block // strip
     held = full[
         lax.div(place, per_block),
@@ -352,18 +398,22 @@
         pl.ds(pl.multiple_of(lax.rem(place, per_block) * strip, strip), strip),
     ]
     pieces[place] = (held.astype(F32).reshape(seqs, strip) + total).astype(BF16)
-    finish(
-        around(
-            n_z, z,
-            lambda k, p: remote(
-                pieces.at[place], pieces.at[place], sems, 11, k, {"tp": 2 * p + core}
-            ),
-        )
-    )
-    side = pl.ds(core * n_z, n_z)
-    copy = remote(pieces.at[side], pieces.at[side], sems, 12, 0, sibling)
-    copy.start()
-    copy.wait()
+    z_copies = around(
+        n_z, z,
+        lambda k, p: remote(
+            pieces.at[place], pieces.at[place], sems, 9, k, {"tp": 2 * p + core}
+        ),
+    )
+    passed = []
+    for i in range(n_z):
+        spot = core * n_z + lax.rem(z + n_z - i, n_z)
+        if i > 0:
+            z_copies[i - 1].wait_recv()
+        passed.append(remote(pieces.at[spot], pieces.at[spot], sems, 10, i, sibling))
+        passed[-1].start()
+    for copy in z_copies:
+        copy.wait_send()
+    finish(passed)
     for i in range(n_tp):
         out[:, i * strip : (i + 1) * strip] = pieces[i]
 
@@ -382,19 +432,20 @@
     any_ = pl.BlockSpec(memory_space=pl.ANY)
     limit = 60 * 1024 * 1024
 
-    proj, gates, spread = pl.pallas_call(
+    proj, gates, top, spread = pl.pallas_call(
         functools.partial(project_kernel, n_ep, n_tp),
         out_shape=(
             jax.ShapeDtypeStruct((seqs, 4 * cols), F32),
             jax.ShapeDtypeStruct((seqs, 2 * heads), F32),
+            jax.ShapeDtypeStruct((heads, seqs), F32),
             jax.ShapeDtypeStruct((n_ep, seqs, block), BF16),
         ),
-        in_specs=[vmem, vmem, any_, any_, any_, any_, any_, any_, vmem],
-        out_specs=(vmem, vmem, vmem),
+        in_specs=[vmem, vmem, any_, any_, any_, any_, any_, any_, vmem, vmem],
+        out_specs=(vmem, vmem, vmem, vmem),
         scratch_shapes=[
             pltpu.VMEM((n_ep, seqs, block), BF16),
             pltpu.VMEM((4, block, cols), BF16),
-            pltpu.VMEM((2, width, heads_all), BF16),
+            pltpu.VMEM((2, heads_all, width), BF16),
             pltpu.VMEM((n_ep, seqs, 4 * cols), BF16),
             pltpu.VMEM((n_ep, seqs, 4 * cols), BF16),
             pltpu.SemaphoreType.DMA((2, n_ep)),
@@ -407,7 +458,7 @@
         name="project",
     )(
         tokens, mixer_gain.reshape(1, width), w_query, w_key, w_value, w_outgate,
-        w_ingate, w_forget, forget_bias.reshape(1, heads_all),
+        w_ingate.T, w_forget.T, forget_bias.reshape(1, heads_all), state_max.T,
     )
 
     group = 8
@@ -418,30 +469,30 @@
             jax.ShapeDtypeStruct((seqs, cols), F32),
             jax.ShapeDtypeStruct(state_matrix.shape, F32),
             jax.ShapeDtypeStruct(state_norm.shape, F32),
-            jax.ShapeDtypeStruct(state_max.shape, F32),
+            jax.ShapeDtypeStruct((heads, seqs), F32),
         ),
         in_specs=[
             pl.BlockSpec((group, 4 * cols), lambda i: (i, 0)),
             pl.BlockSpec((group, 2 * heads), lambda i: (i, 0)),
             pl.BlockSpec((group, heads, size, size), lambda i: (i, 0, 0, 0)),
             pl.BlockSpec((group, heads, size), lambda i: (i, 0, 0)),
-            pl.BlockSpec((group, heads), lambda i: (i, 0)),
+            pl.BlockSpec((heads, seqs), lambda i: (0, 0)),
         ],
         out_specs=(
             pl.BlockSpec((group, cols), lambda i: (i, 0)),
             pl.BlockSpec((group, heads, size, size), lambda i: (i, 0, 0, 0)),
             pl.BlockSpec((group, heads, size), lambda i: (i, 0, 0)),
-            pl.BlockSpec((group, heads), lambda i: (i, 0)),
+            pl.BlockSpec((heads, seqs), lambda i: (0, 0)),
         ),
         name="cell",
-    )(proj, gates, state_matrix, state_norm, state_max)
+    )(proj, gates, state_matrix, state_norm, top)
 
     rows = n_ep * seqs
     chunk = rows // n_tp
     hidden = dense_gate.shape[1]
     strip = width // n_tp
     lanes = -(-(n_ep * expert_gate.shape[0]) // 128) * 128
-    phases, most = 13, max(n_ep, n_tp)
+    phases, most = 11, max(n_ep, n_tp)
     layer_out = pl.pallas_call(
         functools.partial(ffn_kernel, n_ep, n_tp),
         out_shape=jax.ShapeDtypeStruct((seqs, width), BF16),
@@ -454,23 +505,27 @@
         + [
             pltpu.VMEM((n_ep, seqs, cols), BF16),
             pltpu.VMEM((n_ep, seqs, lanes), F32),
-            pltpu.VMEM((n_tp, chunk, block), BF16),
-            pltpu.VMEM((n_tp, chunk, block), BF16),
+            pltpu.VMEM((2, n_tp // 2, chunk, block), BF16),
+            pltpu.VMEM((n_tp // 2, chunk, block), BF16),
+            pltpu.VMEM((n_tp // 2, chunk, block), BF16),
+            pltpu.VMEM((n_tp // 2, chunk, block), BF16),
             pltpu.VMEM((n_ep, n_tp, chunk, block), BF16),
             pltpu.VMEM((n_ep, seqs, 2 * hidden), BF16),
             pltpu.VMEM((n_ep, seqs, 2 * hidden), BF16),
             pltpu.VMEM((n_ep, seqs, hidden), BF16),
             pltpu.VMEM((rows, 128), F32),
-            pltpu.VMEM((rows, block), F32),
             pltpu.VMEM((2, n_ep, seqs, width // 2), BF16),
             pltpu.VMEM((n_ep, seqs, width // 2), BF16),
-            pltpu.VMEM((n_ep, seqs, width // 2), BF16),
-            pltpu.VMEM((n_ep, seqs, width // 2), BF16),
+            pltpu.VMEM((n_tp // 2, n_ep, seqs, strip), BF16),
+            pltpu.VMEM((n_tp // 2, n_ep, seqs, strip), BF16),
             pltpu.VMEM((n_tp // 2, seqs, strip), BF16),
             pltpu.VMEM((n_tp // 2, seqs, strip), BF16),
             pltpu.VMEM((n_tp, seqs, strip), BF16),
             pltpu.SemaphoreType.DMA((phases, most)),
             pltpu.SemaphoreType.DMA((phases, most)),
+        ]
+        + [pltpu.SemaphoreType.DMA((n_tp // 2, n_ep))] * 6
+        + [
             pltpu.SemaphoreType.DMA((7,)),
         ],
         compiler_params=pltpu.CompilerParams(
@@ -479,10 +534,10 @@
         name="feedforward",
     )(
         mixed, spread.reshape(n_tp, chunk, block), ffn_gain.reshape(1, width),
-        w_branch.reshape(1, width), routes, route_weight,
+        w_branch.reshape(1, width), routes.T, route_weight.T,
         w_proj, dense_gate, dense_up, expert_gate, expert_up, dense_down, expert_down,
     )
-    return (layer_out, new_matrix, new_norm, new_max)
+    return (layer_out, new_matrix, new_norm, new_max.T)
 
 
 def solution(mesh):

time: 99 us -> 82.4 us (0.83)
  local copies, waits for them, and re-layouts: 12.1 us -> 2.98 us
  Pallas kernels: 85.8 us -> 78.4 us
    unnamed x9 -> x1, local copies, waits for them, and re-layouts: 10.8 us -> 1.67 us
    pallas_call x1, Pallas kernels: 62.3 us -> 55.4 us  [on_device(): pl.pallas_call(functools.partial(ffn_kernel, n_ep, n_tp), out_shape=jax.S...]
where the time goes in v2:
time: 82.4 us; the launch traced here: 82 us
  Pallas kernels  78.4 us (95%)
  local copies, waits for them, and re-layouts  2.98 us (4%)
    pallas_call x1, Pallas kernels, on_device(): pl.pallas_call(functools.partial(ffn_kernel, n_ep, n_tp), out_shape=jax.S...  55.4 us
    pallas_call x1, Pallas kernels, on_device(): pl.pallas_call(functools.partial(project_kernel, n_ep, n_tp), out_shape=(...  15.6 us
    pallas_call x1, Pallas kernels, on_device(): pl.pallas_call(cell_kernel, grid=(seqs // group,), out_shape=(jax.ShapeDt...  7.48 us
    unnamed x1, local copies, waits for them, and re-layouts  1.67 us

profile of v2, /device:TPU:0, one launch (start us, length us, event | category | flops | bytes accessed | tf_op | source)
XLA Modules:
  0.0 82.0 jit_solution(13112255380301695179)
XLA Ops:
  0.6 1.3 %reshape.27.branch = bf16[1,4096]{1,0:T(2,128)(2,1)} reshape(bf16[4096]{0:T(1024)(128)(2,1)} %param.37) | data formatting | bytes 16384 | tf_op jit(solution)/shard_map/reshape | solution.py:537
  1.9 15.6 %project.1 = (f32[32,1024]{1,0:T(8,128)}, f32[32,4]{1,0:T(8,128)}, f32[2,32]{1,0:T(2,128)}, bf16[4,32,1024]{2,1,0:T(8,128)(2,1)}) custom-call(bf16[32,4096]{1,0:T(8,128)(2,1)} %tokens.1, f32[1,4096]{1,0:T(1,128)} %bitcast.13, bf16[1024,256]{1,0:T(8,128)(2,1)} %w_q.1, bf16[1024,256]{1,0:T(8,128)(2,1)} %w_k.1, bf16[1024,256]{1,0:T(8,128)(2,1)} %w_v.1, ...), custom_call_target="tpu_custom_call" | custom-call | tf_op jit(solution)/shard_map/project/pallas_call | solution.py:435
  17.5 7.5 %cell.1 = (f32[32,256]{1,0:T(8,128)}, f32[32,2,128,128]{3,2,1,0:T(8,128)}, f32[32,2,128]{2,1,0:T(2,128)}, f32[2,32]{1,0:T(2,128)}) custom-call(f32[32,1024]{1,0:T(8,128)} %get-tuple-element.12.proj, f32[32,4]{1,0:T(8,128)} %get-tuple-element.13.gates, f32[32,2,128,128]{3,2,1,0:T(8,128)} %matrix.1, f32[32,2,128]{2,1,0:T(2,128)} %norm.1, ...), custom_call_target="tpu_custom_call" | custom-call | tf_op jit(solution)/shard_map/cell/pallas_call | solution.py:465
  25.0 55.4 %feedforward.1 = bf16[32,4096]{1,0:T(8,128)(2,1)} custom-call(f32[32,256]{1,0:T(8,128)} %get-tuple-element.15.mixed, bf16[8,16,1024]{2,1,0:T(8,128)(2,1)} %bitcast.10, f32[1,4096]{1,0:T(1,128)} %bitcast.14, bf16[1,4096]{1,0:T(2,128)(2,1)} %reshape.27.branch, s32[2,32]{1,0:T(2,128)} %bitcast.16, f32[2,32]{1,0:T(2,128)} %bitcast.17, bf16[256,1024]{1,0:T(8,128)(2,1)} %w_proj.1, ...), custom_call_target="tpu_custom_call" | custom-call | tf_op jit(solution)/shard_map/feedforward/pallas_call | solution.py:496
  80.4 1.7 %copy.28 = bf16[32,4096]{1,0:T(8,128)(2,1)} copy(bf16[32,4096]{1,0:T(8,128)(2,1)} %feedforward.1) | data formatting | bytes 524288
